TPU v7x, 1024 devices: a whole 4x8x16 slice. The times are simulated.
1024 devices in a mesh: sp: 16 (over z), dp: 64 (over y, x, core).
Axes of the slice: x: 4, y: 8, z: 16, core: 2. Of those that a mesh axis runs over, the one named last changes fastest.
Arguments:
- queries: bfloat16 [64, 768, 6144], P('dp', None, 'sp'), may hold values from -64 to 64
- out_grad: bfloat16 [64, 768, 4096], P('dp', None, 'sp'), may hold values from -6 to 6
- latent: bfloat16 [64, 768, 512], P('dp'), may hold values from -6 to 6
- rope_key: bfloat16 [64, 768, 64], P('dp'), may hold values from -6 to 6
- kv_gain: float32 [512], replicated, may hold values from 0.1 to 1.9
- key_up: bfloat16 [512, 4096], P('dp', 'sp'), may hold values from -0.25 to 0.25
- value_up: bfloat16 [512, 4096], P('dp', 'sp'), may hold values from -0.25 to 0.25
Outputs:
- query_grad: bfloat16 [64, 768, 6144], P('dp', None, 'sp')
- latent_grad: bfloat16 [64, 768, 512], P('dp')
- rope_key_grad: bfloat16 [64, 768, 64], P('dp')
- key_up_grad: float32 [512, 4096], P('dp', 'sp')
- value_up_grad: float32 [512, 4096], P('dp', 'sp')
All inputs are finite; a program needn't handle non-finite values.
Results may differ from a plain program's by a relative error of at most 0.019.
The roundings to bfloat16 on the way count: a program that leaves them out, or rounds other values in their place, can miss the bound.
Values may be sent and summed in bfloat16 or wider, within the bound.
A program may use at most 32 MiB of HBM per device.

v0:
```python
import jax
import jax.numpy as jnp
from jax import lax
from jax.sharding import PartitionSpec as P

NOPE_DIM = 128
ROPE_DIM = 64
VALUE_DIM = 128


norm_eps = 1e-06
rope_theta = 10000.0


def in_one_piece(arrays, axis, dim, along):
    ends, at = ([], 0)
    for a in arrays[:-1]:
        at += a.shape[along]
        ends.append(at)
    both = jnp.concatenate(arrays, axis=along)
    return tuple(jnp.split(lax.all_gather(both, axis, axis=dim, tiled=True), ends, axis=along))


def in_one(arrays, axis):
    flat, at, gathered = (jnp.concatenate([a.reshape(-1) for a in arrays]), 0, [])
    subtotal = lax.psum(flat, axis)
    for a in arrays:
        gathered.append(subtotal[at : at + a.size].reshape(a.shape))
        at += a.size
    return tuple(gathered)


def cut_along(x, dim, peers):
    dims = x.shape
    pieces = x.reshape(*dims[:dim], peers, dims[dim] // peers, *dims[dim + 1 :])
    return jnp.moveaxis(pieces, dim, 0)


def sent_and_summed(x, axis, dim):
    peers = lax.axis_size(axis)
    pieces = lax.all_to_all(cut_along(x, dim, peers), axis, 0, 0, tiled=True)
    return jnp.sum(pieces, axis=0)


def rope_tables(length, width):
    half_width = width // 2
    frequency = rope_theta ** (-(jnp.arange(half_width, dtype=jnp.float32) * 2.0 / width))
    position = jnp.arange(length, dtype=jnp.int32).astype(jnp.float32)
    angles = position[:, None] * frequency[None, :]
    return (jnp.cos(angles), jnp.sin(angles))


def rotate(tensor, cosine, sine_table):
    half_width = tensor.shape[-1] // 2
    first_half = tensor[..., :half_width]
    second = tensor[..., half_width:]
    return jnp.concatenate(
        [first_half * cosine - second * sine_table, second * cosine + first_half * sine_table],
        axis=-1,
    )


def unrotate(upstream, cosine, sine_table):
    half_width = upstream.shape[-1] // 2
    first_half = upstream[..., :half_width]
    second = upstream[..., half_width:]
    return jnp.concatenate(
        [first_half * cosine + second * sine_table, second * cosine - first_half * sine_table],
        axis=-1,
    )


def head_backward(query_used, key_used, head_value, head_grad, score_scale):
    length = query_used.shape[0]
    scores = jnp.dot(query_used, key_used.T, preferred_element_type=jnp.float32) * score_scale
    causal = lax.broadcasted_iota(jnp.int32, (length, length), 0) >= lax.broadcasted_iota(
        jnp.int32, (length, length), 1
    )
    scores = jnp.where(causal, scores, -jnp.inf)
    row_top = jnp.max(scores, axis=1, keepdims=True)
    weights = jnp.exp(scores - row_top)
    probs = weights / jnp.sum(weights, axis=1, keepdims=True)
    probs_low = probs.astype(jnp.bfloat16)
    value_grad = jnp.dot(probs_low.T, head_grad, preferred_element_type=jnp.float32).astype(
        jnp.bfloat16
    )
    prob_grad = jnp.dot(head_grad, head_value.T, preferred_element_type=jnp.float32)
    center = jnp.sum(probs * prob_grad, axis=1, keepdims=True)
    score_grad = (probs * (prob_grad - center) * score_scale).astype(jnp.bfloat16)
    query_grad = jnp.dot(score_grad, key_used, preferred_element_type=jnp.float32)
    key_grad = jnp.dot(score_grad.T, query_used, preferred_element_type=jnp.float32)
    return (query_grad, key_grad, value_grad)


def attend(queries, head_grads, keys, values, key_rot, cosine, sine_table):
    length = queries.shape[0]
    head_count = head_grads.shape[1] // VALUE_DIM
    qk_width = NOPE_DIM + ROPE_DIM
    query_heads = queries.reshape(length, head_count, qk_width)
    rotated = rotate(
        query_heads[:, :, NOPE_DIM:].astype(jnp.float32), cosine[:, None, :], sine_table[:, None, :]
    ).astype(jnp.bfloat16)
    query_used = jnp.concatenate([query_heads[:, :, :NOPE_DIM], rotated], axis=-1).transpose(
        1, 0, 2
    )
    key_heads = keys.reshape(length, head_count, NOPE_DIM).transpose(1, 0, 2)
    key_used = jnp.concatenate(
        [key_heads, jnp.broadcast_to(key_rot[None], (head_count, length, ROPE_DIM))], axis=-1
    )
    value_heads = values.reshape(length, head_count, VALUE_DIM).transpose(1, 0, 2)
    grad_heads = head_grads.reshape(length, head_count, VALUE_DIM).transpose(1, 0, 2)
    score_scale = qk_width ** (-0.5)
    query_part, key_part, value_part = lax.map(
        lambda items: head_backward(items[0], items[1], items[2], items[3], score_scale),
        (query_used, key_used, value_heads, grad_heads),
    )
    query_rot_grad = unrotate(query_part[:, :, NOPE_DIM:], cosine[None], sine_table[None])
    query_grad = jnp.concatenate([query_part[:, :, :NOPE_DIM], query_rot_grad], axis=-1).astype(
        jnp.bfloat16
    )
    query_grad = query_grad.transpose(1, 0, 2).reshape(length, head_count * qk_width)
    key_plain_grad = (
        key_part[:, :, :NOPE_DIM]
        .astype(jnp.bfloat16)
        .transpose(1, 0, 2)
        .reshape(length, head_count * NOPE_DIM)
    )
    key_rot_grad = jnp.sum(key_part[:, :, NOPE_DIM:], axis=0)
    value_grad = value_part.transpose(1, 0, 2).reshape(length, head_count * VALUE_DIM)
    return (query_grad, key_plain_grad, key_rot_grad, value_grad)


def finish(comp_total, rot_total, raw_latent, inverse, kv_gain, cosine, sine_table):
    mixed = comp_total * kv_gain
    spread = jnp.mean(raw_latent * mixed, axis=-1, keepdims=True)
    latent_grad = (inverse * mixed - raw_latent * inverse**3 * spread).astype(jnp.bfloat16)
    rope_grad = unrotate(rot_total, cosine, sine_table).astype(jnp.bfloat16)
    return (latent_grad, rope_grad)


def shards(queries, out_grad, latent, rope_key, kv_gain, key_up, value_up):
    key_whole, value_whole = in_one_piece((key_up, value_up), "dp", 0, 1)
    batch_count, seq_count, latent_width = latent.shape
    raw_latent = latent.astype(jnp.float32)
    inverse = lax.rsqrt(jnp.mean(raw_latent * raw_latent, axis=-1, keepdims=True) + norm_eps)
    compressed = (raw_latent * inverse * kv_gain).astype(jnp.bfloat16)
    cosine, sine_table = rope_tables(seq_count, ROPE_DIM)
    key_rot = rotate(rope_key.astype(jnp.float32), cosine, sine_table).astype(jnp.bfloat16)
    flat_comp = compressed.reshape(batch_count * seq_count, latent_width)
    keys = jnp.dot(flat_comp, key_whole, preferred_element_type=jnp.float32).astype(jnp.bfloat16)
    values = jnp.dot(flat_comp, value_whole, preferred_element_type=jnp.float32).astype(
        jnp.bfloat16
    )
    keys = keys.reshape(batch_count, seq_count, key_whole.shape[1])
    values = values.reshape(batch_count, seq_count, value_whole.shape[1])

    def per_sequence(items):
        query_grad, key_plain_grad, key_rot_grad, value_grad = attend(
            items[0], items[1], items[2], items[3], items[4], cosine, sine_table
        )
        comp_part = jnp.dot(
            key_plain_grad, key_whole.T, preferred_element_type=jnp.float32
        ) + jnp.dot(value_grad, value_whole.T, preferred_element_type=jnp.float32)
        return (query_grad, key_plain_grad, value_grad, comp_part, key_rot_grad)

    query_grad, key_plain_grad, value_grad, comp_part, rot_part = lax.map(
        per_sequence, (queries, out_grad, keys, values, key_rot)
    )
    grad_pair = jnp.concatenate([key_plain_grad, value_grad], axis=-1).reshape(
        batch_count * seq_count, -1
    )
    grad_scale = float(lax.axis_size("dp") * batch_count * seq_count) ** (-0.5)
    comp_total, rot_total = tuple(
        (
            part.astype(jnp.float32)
            for part in in_one(
                (comp_part.astype(jnp.bfloat16), rot_part.astype(jnp.bfloat16)), "sp"
            )
        )
    )
    latent_grad, rope_grad = finish(
        comp_total, rot_total, raw_latent, inverse, kv_gain, cosine, sine_table
    )
    product = lax.dot_general(
        flat_comp, grad_pair, (((0,), (0,)), ((), ())), preferred_element_type=jnp.float32
    )
    combined = sent_and_summed(product * grad_scale, "dp", 0)
    split_at = key_up.shape[1]
    return (query_grad, latent_grad, rope_grad, combined[:, :split_at], combined[:, split_at:])


def solution(mesh):
    return jax.shard_map(
        shards,
        mesh=mesh,
        in_specs=(
            P("dp", None, "sp"),
            P("dp", None, "sp"),
            P("dp", None, None),
            P("dp", None, None),
            P(),
            P("dp", "sp"),
            P("dp", "sp"),
        ),
        out_specs=(
            P("dp", None, "sp"),
            P("dp", None, None),
            P("dp", None, None),
            P("dp", "sp"),
            P("dp", "sp"),
        ),
        check_vma=False,
    )
```

profile of v0, /device:TPU:6, one launch (start us, length us, event | category | flops | bytes accessed | tf_op | source)
XLA Modules:
  0.0 260.1 jit_solution(10246196345459458051)
XLA Ops:
  7.3 1.4 copy.39
  9.0 60.2 %all_gather.3 = bf16[512,512]{1,0:T(8,128)(2,1)S(1)} all-gather(bf16[8,512]{1,0:T(8,128)(2,1)S(1)} %pad_maximum_fusion.5), channel_id=1, replica_groups=mesh['sp'=16,'dp'=64] {'dp'}, dimensions={0}, use_global_device_ids=true | all-gather | bytes 532480 | tf_op jit(solution)/shard_map/all_gather | solution.py:21
  72.0 0.9 copy.43
  72.9 0.9 copy.42
  74.1 0.9 maximum_bitcast_fusion.2
  75.0 20.0 %while.19 = (s32[]{:T(128)}, f32[2,768,192]{1,2,0:T(8,128)}, f32[2,768,192]{1,2,0:T(8,128)}, bf16[2,768,128]{1,2,0:T(8,128)(2,1)}, bf16[2,768,192]{1,2,0:T(8,128...) while((s32[]{:T(128)}, f32[2,768,192]{1,2,0:T(8,128)}, ...), condition=%wide.region_5.6_spmd, body=%wide.region_1.5_spmd.sunk | while | flops 992769792 | bytes 47030024 | solution.py:113
  75.0 1.5 fusion.96
  78.1 0.7 constant_dynamic-update-slice_fusion.2
  78.8 1.6 multiply_reduce_fusion.2
  82.5 1.0 copy-done.13
  83.9 1.0 copy-done.10
  85.0 1.5 fusion.96
  86.8 0.6 copy-done.15
  88.1 0.7 constant_dynamic-update-slice_fusion.2
  88.8 1.6 multiply_reduce_fusion.2
  92.5 1.0 copy-done.13
  93.9 1.0 copy-done.10
  95.0 1.3 slice.139
  96.2 1.0 slice_reduce_fusion
  97.3 1.4 fusion.47
  99.8 1.0 pad_maximum_fusion
  100.8 1.9 fusion.40
  102.6 6.3 %all-to-all-start = ((f32[64,8,512]{2,1,0:T(8,128)}), f32[64,8,512]{2,1,0:T(8,128)S(1)}, u32[]{:S(2)}, u32[]{:S(2)}) async-start(f32[64,8,512]{2,1,0:T(8,128)} %fusion.40), calls=%async_computation | async-start | bytes 2097152 | tf_op jit(solution)/shard_map/all_to_all | solution.py:41
  109.2 1.1 copy.50
  110.2 132.6 %all-reduce.2.cloned.1.call-done = bf16[442368]{0:T(1024)(128)(2,1)} async-done(((bf16[442368]{0:T(1024)(128)(2,1)}), bf16[442368]{0:T(1024)(128)(2,1)}) %all-reduce.2.cloned.1.call-update) | async-done | bytes 884752 | tf_op jit(solution)/shard_map/psum | solution.py:26
  242.8 2.4 slice_convert_fusion
  245.2 0.9 slice_convert_fusion.4
  246.6 0.8 copy.56
  247.4 1.5 reshape.350
  248.9 1.3 fusion.63
  250.3 0.6 pad_maximum_fusion.4
  251.2 1.3 fusion.38
  (109 shorter events, 13.4 us)
Async XLA Ops:
  7.2 1.6 copy-start.1
  7.2 235.6 %all-reduce.2.cloned.1.call-start = ((), (), s32[]{:S(2)}) async-start(), calls=%async_computation.1 | async-start | bytes 1769472 | tf_op jit(solution)/shard_map/psum | solution.py:26
  7.2 63.9 %copy-start.22 = (f32[32]{0:T(128)}, f32[32]{0:T(128)S(1)}, u32[]{:S(2)}) copy-start(f32[32]{0:T(128)S(1)} %negate_power_fusion) | copy-start | bytes 388
  7.3 1.7 copy-start.24
  7.3 1.7 copy-start.25
  8.6 60.6 %copy-start.20 = (f32[512]{0:T(512)S(1)}, f32[512]{0:T(512)}, u32[]{:S(2)}) copy-start(f32[512]{0:T(512)} %param.13) | copy-start | bytes 6148
  9.0 61.6 %copy-start.18 = (f32[768]{0:T(1024)}, f32[768]{0:T(1024)S(1)}, u32[]{:S(2)}) copy-start(f32[768]{0:T(1024)S(1)} %get-tuple-element.171) | copy-start | bytes 9220
  69.3 1.4 copy-start.17
  70.6 2.3 copy-start.14
  71.1 2.9 %copy-start.5 = (f32[768,32]{0,1:T(8,128)}, f32[768,32]{0,1:T(8,128)S(1)}, u32[]{:S(2)}) copy-start(f32[768,32]{0,1:T(8,128)S(1)} %get-tuple-element.168) | copy-start | bytes 294916
  71.1 2.9 %copy-start.7 = (f32[768,32]{0,1:T(8,128)}, f32[768,32]{0,1:T(8,128)S(1)}, u32[]{:S(2)}) copy-start(f32[768,32]{0,1:T(8,128)S(1)} %get-tuple-element.169) | copy-start | bytes 294916
  80.4 1.1 copy-start
  80.4 1.4 copy-start.12
  81.1 2.4 copy-start.9
  82.4 1.0 copy-start.13
  83.9 1.1 copy-start.10
  86.5 1.0 copy-start.15
  90.4 1.1 copy-start
  90.4 1.4 copy-start.12
  91.1 2.4 copy-start.9
  92.4 1.0 copy-start.13
  93.9 1.1 copy-start.10
  95.0 3.7 %copy-start.4 = (bf16[512,512]{1,0:T(8,128)(2,1)S(1)}, bf16[512,512]{1,0:T(8,128)(2,1)}, u32[]{:S(2)}) copy-start(bf16[512,512]{1,0:T(8,128)(2,1)} %copy-done.3) | copy-start | bytes 1572868
  95.0 3.7 %copy-start.16 = (bf16[2,768,128]{1,2,0:T(8,128)(2,1)S(1)}, bf16[2,768,128]{1,2,0:T(8,128)(2,1)}, u32[]{:S(2)}) copy-start(bf16[2,768,128]{1,2,0:T(8,128)(2,1)} %get-tuple-element.96) | copy-start | bytes 1179652
  99.4 1.3 copy-start.2
  99.4 1.3 copy-start.19
  99.4 1.3 copy-start.21
  102.6 6.3 %copy-start.11 = (f32[2,768,192]{1,2,0:T(8,128)S(1)}, f32[2,768,192]{1,2,0:T(8,128)}, u32[]{:S(2)}) copy-start(f32[2,768,192]{1,2,0:T(8,128)} %get-tuple-element.94) | copy-start | bytes 3538948
  102.6 6.4 %copy-start.6 = (f32[768,32]{0,1:T(8,128)S(1)}, f32[768,32]{0,1:T(8,128)}, u32[]{:S(2)}) copy-start(f32[768,32]{0,1:T(8,128)} %copy-done.5) | copy-start | bytes 294916
  102.6 6.4 %copy-start.8 = (f32[768,32]{0,1:T(8,128)S(1)}, f32[768,32]{0,1:T(8,128)}, u32[]{:S(2)}) copy-start(f32[768,32]{0,1:T(8,128)} %copy-done.7) | copy-start | bytes 294916
  102.6 149.9 %all-to-all-start = ((f32[64,8,512]{2,1,0:T(8,128)}), f32[64,8,512]{2,1,0:T(8,128)S(1)}, u32[]{:S(2)}, u32[]{:S(2)}) async-start(f32[64,8,512]{2,1,0:T(8,128)} %fusion.40), calls=%async_computation | async-start | bytes 2097152 | tf_op jit(solution)/shard_map/all_to_all | solution.py:41
  247.4 1.5 copy-start.23
  (2 other events, 1.8 us)
Sparse Core Ops, SparseCore 0:
  100.9 141.9 all-reduce.1
where the time goes:
time: 261 us; the launch traced here: 260 us
  waiting for transfers between devices  133 us (51%)
  blocking collectives  60.2 us (23%)
  local copies, waits for them, and re-layouts  19 us (7%)
  between operations  14.5 us (6%)
  matrix products  13.9 us (5%)
  other arithmetic  13.3 us (5%)
  starting transfers between devices  6.35 us (2%)
    psum x1, waiting for transfers between devices, in_one(): subtotal = lax.psum(flat, axis)  133 us
    all_gather x1, blocking collectives, in_one_piece(): lax.all_gather(both, axis, axis=dim, tiled=True)  60.2 us
    while x24, local copies, waits for them, and re-layouts  7.02 us
    all_to_all x1, starting transfers between devices, sent_and_summed(): pieces = lax.all_to_all(cut_along(x, dim, peers), axis, 0, 0, tiled=True)  6.32 us
  transfers between devices with their start and end apart: 2, of which 1 were waited for; matrix products, arithmetic and copies ran while one was open for 5% of the time, Pallas kernels for 0%

commit v1 on v0

v1 whole, which is shorter than its diff:
```python
import jax
import jax.numpy as jnp
import numpy as np
from jax import lax
from jax.experimental import pallas as pl
from jax.experimental.pallas import tpu as pltpu
from jax.sharding import PartitionSpec as P

MESH = pl.DeviceIdType.MESH
F32 = jnp.float32
BF16 = jnp.bfloat16

NX, NY, NC, NZ = 4, 8, 2, 16
SEQ = 768
LAT = 512
BLK = 256
NB = SEQ // BLK
HEADS = 2
SUB = BLK // NZ
WID = 640
NORM_EPS = 1e-06
SCORE_SCALE = 192 ** (-0.5)
LOG2E = 1.4426950408889634
GRAD_SCALE = 49152.0 ** (-0.5)


def rope_tables():
    steps = np.arange(32, dtype=np.float32) * np.float32(2.0) / np.float32(64)
    frequency = np.power(np.float32(10000.0), -steps).astype(np.float32)
    position = np.arange(SEQ, dtype=np.float32)
    angles = (position[:, None] * frequency[None, :]).astype(np.float32).astype(np.float64)
    cosine = np.cos(angles).astype(np.float32)
    sine = np.sin(angles).astype(np.float32)
    return (
        np.concatenate([cosine] * 4, axis=1),
        np.concatenate([-sine, sine, -sine, sine], axis=1),
    )


def lanes(shape):
    return lax.broadcasted_iota(jnp.int32, shape, len(shape) - 1)


def partner(t):
    lane = lanes(t.shape)
    axis = len(t.shape) - 1
    return jnp.where((lane % 64) < 32, pltpu.roll(t, 96, axis), pltpu.roll(t, 32, axis))


def turn(t, cosine, sine):
    return t * cosine + partner(t) * sine


def unturn(t, cosine, sine):
    return t * cosine - partner(t) * sine


def dot(a, b, dims):
    return lax.dot_general(a, b, (dims, ((), ())), preferred_element_type=F32)


NT = ((1,), (1,))
NN = ((1,), (0,))
TN = ((0,), (0,))


def kernel(
    q_ref, do_ref, lat_ref, rk_ref, gain_ref, ku_ref, vu_ref, cos_ref, sin_ref,
    qg_ref, lg_ref, rg_ref, kg_ref, vg_ref,
    gbuf, wk, wv, comp, q2, k2, v2, dk, dv, kpl, vgr,
    part, sb_r, rb_r, sb_l, rb_l, outb,
    gs, rc, hs, rx, ys, ry,
    sy, ry_sem, sx, rx_sem, sc, rc_sem,
    s_r, r_r, s_l, r_l, as_r, ar_r, as_l, ar_l,
    gsc, grc, gsx, grx, gsy, gry,
):
    z = lax.axis_index("sp")
    me = lax.axis_index("dp")
    c = lax.rem(me, NC)
    x = lax.rem(me // NC, NX)
    y = me // (NC * NX)

    def at(yy, xx, cc):
        return (z, (yy * NX + xx) * NC + cc)

    right = (lax.rem(z + 1, NZ), me)
    left = (lax.rem(z + NZ - 1, NZ), me)

    def other_y(k):
        return lax.rem(y + k, NY)

    def other_x(k):
        return lax.rem(x + k, NX)

    def remote(src, dst, send, recv, dev):
        return pltpu.make_async_remote_copy(
            src_ref=src, dst_ref=dst, send_sem=send, recv_sem=recv,
            device_id=dev, device_id_type=MESH,
        )

    barrier = pltpu.get_barrier_semaphore()
    for k in range(1, NY):
        pl.semaphore_signal(barrier, inc=1, device_id=at(other_y(k), x, c), device_id_type=MESH)
    for k in range(1, NX):
        pl.semaphore_signal(barrier, inc=1, device_id=at(y, other_x(k), c), device_id_type=MESH)
    pl.semaphore_signal(barrier, inc=1, device_id=at(y, x, 1 - c), device_id_type=MESH)
    pl.semaphore_signal(barrier, inc=1, device_id=right, device_id_type=MESH)
    pl.semaphore_signal(barrier, inc=1, device_id=left, device_id_type=MESH)
    pl.semaphore_wait(barrier, NY - 1 + NX - 1 + 3)

    gbuf[c, x, y] = jnp.concatenate(
        [ku_ref[...].astype(F32), vu_ref[...].astype(F32)], axis=0
    ).astype(BF16)

    def wcopy_y(k):
        return remote(gbuf.at[c, x, y], gbuf.at[c, x, y], sy.at[k], ry_sem.at[k], at(other_y(k), x, c))

    def wcopy_x(k):
        return remote(gbuf.at[c, x], gbuf.at[c, x], sx.at[k], rx_sem.at[k], at(y, other_x(k), c))

    def wcopy_c(k):
        xx = other_x(k)
        return remote(gbuf.at[c, xx], gbuf.at[c, xx], sc.at[k], rc_sem.at[k], at(y, x, 1 - c))

    for k in range(1, NY):
        wcopy_y(k).start()

    raw = lat_ref[...].astype(F32)
    inverse = lax.rsqrt(jnp.mean(raw * raw, axis=-1, keepdims=True) + NORM_EPS)
    comp[...] = (raw * inverse * gain_ref[...]).astype(BF16)
    cosine, sine = cos_ref[...], sin_ref[...]
    lane = lanes((SEQ, 128))
    low = lane < 64
    t1 = q_ref[:, 128:256].astype(F32)
    t1 = jnp.where(low, turn(t1, cosine, sine), t1).astype(BF16)
    t2 = q_ref[:, 256:384].astype(F32)
    t2 = jnp.where(low, t2, turn(t2, cosine, sine)).astype(BF16)
    q2[0, :, :128] = q_ref[:, :128]
    q2[0, :, 128:] = t1
    q2[1, :, :128] = t1
    q2[1, :, 128:] = t2
    key = rk_ref[...].astype(F32)
    key = turn(jnp.concatenate([key, key], axis=1), cosine, sine)
    k2[0, :, 128:] = jnp.where(low, key, 0.0).astype(BF16)

    for k in range(1, NY):
        wcopy_y(k).wait_recv()
    for k in range(1, NX):
        wcopy_x(k).start()
    wcopy_c(0).start()
    for k in (1, 3, 2):
        wcopy_x(k).wait_recv()
        wcopy_c(NX - k).start()
    for k in range(NX):
        wcopy_c(k).wait_recv()
    for k in range(1, NY):
        wcopy_y(k).wait_send()
    for k in range(1, NX):
        wcopy_x(k).wait_send()
    for k in range(NX):
        wcopy_c(k).wait_send()

    def place(i, _):
        g0 = gbuf[0, lax.rem(i, NX), i // NX].astype(F32)
        g1 = gbuf[1, lax.rem(i, NX), i // NX].astype(F32)
        rows = pl.ds(pl.multiple_of(i * 16, 16), 16)
        wk[rows, :] = jnp.concatenate([g0[:8], g1[:8]], axis=0).astype(BF16)
        wv[rows, :] = jnp.concatenate([g0[8:], g1[8:]], axis=0).astype(BF16)
        return 0

    lax.fori_loop(0, NX * NY, place, 0)

    keys = dot(comp[...], wk[...], NN)
    k2[0, :, :128] = keys[:, :128].astype(BF16)
    shifted = pltpu.roll(keys[:, 128:], 64, 1)
    k2[1, :, :128] = jnp.where(low, 0.0, shifted).astype(BF16)
    k2[1, :, 128:] = jnp.where(low, shifted, key).astype(BF16)
    v2[...] = dot(comp[...], wv[...], NN).astype(BF16)

    def first_r(j):
        return remote(part.at[j, lax.rem(z + 8, NZ)], rb_r.at[0, j], s_r.at[0, j], r_r.at[0, j], right)

    def first_l(j):
        return remote(part.at[j, lax.rem(z + NZ - 7, NZ)], rb_l.at[0, j], s_l.at[0, j], r_l.at[0, j], left)

    def next_r(s, j):
        return remote(sb_r.at[s, j], rb_r.at[s, j], s_r.at[s, j], r_r.at[s, j], right)

    def next_l(s, j):
        return remote(sb_l.at[s, j], rb_l.at[s, j], s_l.at[s, j], r_l.at[s, j], left)

    for i in reversed(range(NB)):
        n = (i + 1) * BLK
        rows = slice(i * BLK, n)
        qgs = []
        for h in range(HEADS):
            qi = q2[h, rows, :]
            doi = do_ref[rows, h * 128 : (h + 1) * 128]
            scores = dot(k2[h, :n, :], qi, NT)
            kpos = lax.broadcasted_iota(jnp.int32, (n, BLK), 0)
            qpos = lax.broadcasted_iota(jnp.int32, (n, BLK), 1) + i * BLK
            scores = jnp.where(kpos <= qpos, scores, -jnp.inf)
            top = jnp.max(scores, axis=0, keepdims=True)
            weights = jnp.exp2((scores - top) * (SCORE_SCALE * LOG2E))
            probs = weights * (1.0 / jnp.sum(weights, axis=0, keepdims=True))
            pgrad = dot(v2[:n, h * 128 : (h + 1) * 128], doi, NT)
            center = jnp.sum(probs * pgrad, axis=0, keepdims=True)
            sgrad = (probs * (pgrad - center) * SCORE_SCALE).astype(BF16)
            dvi = dot(probs.astype(BF16), doi, NN)
            dki = dot(sgrad, qi, NN)
            if i == NB - 1:
                dv[h] = dvi
                dk[h] = dki
            else:
                dv[h, :n, :] += dvi
                dk[h, :n, :] += dki
            qgs.append(dot(sgrad, k2[h, :n, :], TN))
        lowb = lanes((BLK, 128)) < 64
        cb, sbk = cos_ref[rows, :], sin_ref[rows, :]
        qg_ref[rows, :128] = qgs[0][:, :128].astype(BF16)
        g1 = qgs[0][:, 128:] + qgs[1][:, :128]
        qg_ref[rows, 128:256] = jnp.where(lowb, unturn(g1, cb, sbk), g1).astype(BF16)
        g2 = qgs[1][:, 128:]
        qg_ref[rows, 256:] = jnp.where(lowb, g2, unturn(g2, cb, sbk)).astype(BF16)

        ka, kb = dk[0, rows, :128], dk[0, rows, 128:]
        la, lb = dk[1, rows, :128], dk[1, rows, 128:]
        kp1 = pltpu.roll(jnp.where(lowb, lb, la), 64, 1)
        kp = jnp.concatenate([ka, kp1], axis=1).astype(BF16)
        vb = jnp.concatenate([dv[0, rows, :], dv[1, rows, :]], axis=1).astype(BF16)
        kpl[rows, :] = kp
        vgr[rows, :] = vb
        rot = jnp.where(lowb, kb + pltpu.roll(lb, 64, 1), 0.0)
        lat = dot(kp, wk[...], NT) + dot(vb, wv[...], NT)
        part[i, :, :, :LAT] = lat.astype(BF16).reshape(NZ, SUB, LAT)
        part[i, :, :, LAT:] = rot.astype(BF16).reshape(NZ, SUB, 128)
        first_r(i).start()
        first_l(i).start()

    pk = dot(comp[...], kpl[...], TN).reshape(NX * NY, 2, 8, 256)
    pv = dot(comp[...], vgr[...], TN).reshape(NX * NY, 2, 8, 256)
    for cc in range(NC):
        both = jnp.concatenate([pk[:, cc], pv[:, cc]], axis=1).astype(BF16)
        for yy in range(NY):
            for xx in range(NX):
                gs[cc, xx, yy] = both[yy * NX + xx]
    gcore = remote(gs.at[1 - c], rc, gsc, grc, at(y, x, 1 - c))
    gcore.start()

    def hop_r(s, j):
        next_owner = lax.rem(z + 7 - s, NZ)
        next_r(s, j).wait_recv()
        sb_r[s + 1, j] = (rb_r[s, j].astype(F32) + part[j, next_owner].astype(F32)).astype(BF16)
        next_r(s + 1, j).start()

    def hop_l(s, j):
        next_owner = lax.rem(z + NZ - 6 + s, NZ)
        next_l(s, j).wait_recv()
        sb_l[s + 1, j] = (rb_l[s, j].astype(F32) + part[j, next_owner].astype(F32)).astype(BF16)
        next_l(s + 1, j).start()

    order = tuple(reversed(range(NB)))

    def hops(s, _):
        for j in order:
            hop_r(s, j)
            hop_l(s, j)
        return 0

    lax.fori_loop(0, 1, hops, 0)

    gcore.wait_recv()
    for xx in range(NX):
        hs[xx] = (gs[c, xx].astype(F32) + rc[xx].astype(F32)).astype(BF16)

    def gcopy_x(k):
        return remote(hs.at[other_x(k)], rx.at[k], gsx.at[k], grx.at[k], at(y, other_x(k), c))

    for k in range(1, NX):
        gcopy_x(k).start()

    lax.fori_loop(1, 4, hops, 0)

    total = hs[x].astype(F32)
    for k in range(1, NX):
        gcopy_x(k).wait_recv()
        total += rx[k].astype(F32)
    ys[...] = total.astype(BF16)

    def gcopy_y(k):
        return remote(ys.at[other_y(k)], ry.at[k], gsy.at[k], gry.at[k], at(other_y(k), x, c))

    for k in range(1, NY):
        gcopy_y(k).start()

    lax.fori_loop(4, 6, hops, 0)
    for j in order:
        hop_r(6, j)

    def ag_r(s, j):
        o = lax.rem(z + NZ - s, NZ)
        return remote(outb.at[j, o], outb.at[j, o], as_r.at[s, j], ar_r.at[s, j], right)

    def ag_l(s, j):
        o = lax.rem(z + s, NZ)
        return remote(outb.at[j, o], outb.at[j, o], as_l.at[s, j], ar_l.at[s, j], left)

    for j in order:
        next_l(6, j).wait_recv()
        next_r(7, j).wait_recv()
        own = part[j, z].astype(F32) + rb_r[7, j].astype(F32) + rb_l[6, j].astype(F32)
        at_rows = pl.ds(pl.multiple_of(j * BLK + z * SUB, SUB), SUB)
        rw = lat_ref[at_rows, :].astype(F32)
        inv = lax.rsqrt(jnp.mean(rw * rw, axis=-1, keepdims=True) + NORM_EPS)
        u = own[:, :LAT] * gain_ref[...]
        spread = jnp.mean(rw * u, axis=-1, keepdims=True)
        outb[j, z, :, :LAT] = (inv * u - rw * (inv * inv * inv) * spread).astype(BF16)
        outb[j, z, :, LAT:] = unturn(own[:, LAT:], cos_ref[at_rows, :], sin_ref[at_rows, :]).astype(BF16)
        ag_r(0, j).start()
        ag_l(0, j).start()

    acc = ys[y].astype(F32)
    for k in range(1, NY):
        gcopy_y(k).wait_recv()
        acc += ry[k].astype(F32)
    acc = acc * GRAD_SCALE
    kg_ref[...] = acc[:8]
    vg_ref[...] = acc[8:]

    def relay(s, _):
        for j in order:
            ag_r(s, j).wait_recv()
            ag_r(s + 1, j).start()
            ag_l(s, j).wait_recv()
            ag_l(s + 1, j).start()
        return 0

    lax.fori_loop(0, 6, relay, 0)
    for j in order:
        ag_r(6, j).wait_recv()
        ag_r(7, j).start()
        ag_l(6, j).wait_recv()
    for j in order:
        ag_r(7, j).wait_recv()

    for j in range(NB):
        block = outb[j]
        lg_ref[j * BLK : (j + 1) * BLK, :] = block[:, :, :LAT].reshape(BLK, LAT)
        rg_ref[j * BLK : (j + 1) * BLK, :] = block[:, :, LAT : LAT + 64].reshape(BLK, 64)

    gcore.wait_send()
    for k in range(1, NX):
        gcopy_x(k).wait_send()
    for k in range(1, NY):
        gcopy_y(k).wait_send()
    for j in range(NB):
        first_r(j).wait_send()
        first_l(j).wait_send()

    def sent_r(s, _):
        for j in range(NB):
            next_r(s, j).wait_send()
        return 0

    def sent_l(s, _):
        for j in range(NB):
            next_l(s, j).wait_send()
        return 0

    def asent_r(s, _):
        for j in range(NB):
            ag_r(s, j).wait_send()
        return 0

    def asent_l(s, _):
        for j in range(NB):
            ag_l(s, j).wait_send()
        return 0

    lax.fori_loop(1, 8, sent_r, 0)
    lax.fori_loop(1, 7, sent_l, 0)
    lax.fori_loop(0, 8, asent_r, 0)
    lax.fori_loop(0, 7, asent_l, 0)


def shards(queries, out_grad, latent, rope_key, kv_gain, key_up, value_up):
    cosine, sine = rope_tables()
    vmem = pl.BlockSpec(memory_space=pltpu.VMEM)
    dma = pltpu.SemaphoreType.DMA
    outs = pl.pallas_call(
        kernel,
        out_shape=(
            jax.ShapeDtypeStruct((SEQ, 384), BF16),
            jax.ShapeDtypeStruct((SEQ, LAT), BF16),
            jax.ShapeDtypeStruct((SEQ, 64), BF16),
            jax.ShapeDtypeStruct((8, 256), F32),
            jax.ShapeDtypeStruct((8, 256), F32),
        ),
        in_specs=[vmem] * 9,
        out_specs=(vmem,) * 5,
        scratch_shapes=[
            pltpu.VMEM((NC, NX, NY, 16, 256), BF16),
            pltpu.VMEM((LAT, 256), BF16),
            pltpu.VMEM((LAT, 256), BF16),
            pltpu.VMEM((SEQ, LAT), BF16),
            pltpu.VMEM((HEADS, SEQ, 256), BF16),
            pltpu.VMEM((HEADS, SEQ, 256), BF16),
            pltpu.VMEM((SEQ, 256), BF16),
            pltpu.VMEM((HEADS, SEQ, 256), F32),
            pltpu.VMEM((HEADS, SEQ, 128), F32),
            pltpu.VMEM((SEQ, 256), BF16),
            pltpu.VMEM((SEQ, 256), BF16),
            pltpu.VMEM((NB, NZ, SUB, WID), BF16),
            pltpu.VMEM((8, NB, SUB, WID), BF16),
            pltpu.VMEM((8, NB, SUB, WID), BF16),
            pltpu.VMEM((7, NB, SUB, WID), BF16),
            pltpu.VMEM((7, NB, SUB, WID), BF16),
            pltpu.VMEM((NB, NZ, SUB, WID), BF16),
            pltpu.VMEM((NC, NX, NY, 16, 256), BF16),
            pltpu.VMEM((NX, NY, 16, 256), BF16),
            pltpu.VMEM((NX, NY, 16, 256), BF16),
            pltpu.VMEM((NX, NY, 16, 256), BF16),
            pltpu.VMEM((NY, 16, 256), BF16),
            pltpu.VMEM((NY, 16, 256), BF16),
            dma((NY,)), dma((NY,)), dma((NX,)), dma((NX,)), dma((NX,)), dma((NX,)),
            dma((8, NB)), dma((8, NB)), dma((7, NB)), dma((7, NB)),
            dma((8, NB)), dma((8, NB)), dma((7, NB)), dma((7, NB)),
            dma, dma, dma((NX,)), dma((NX,)), dma((NY,)), dma((NY,)),
        ],
        compiler_params=pltpu.CompilerParams(collective_id=0, has_side_effects=True),
    )(
        queries[0], out_grad[0], latent[0], rope_key[0], kv_gain[None], key_up, value_up,
        jnp.asarray(cosine), jnp.asarray(sine),
    )
    query_grad, latent_grad, rope_grad, key_grad, value_grad = outs
    return (query_grad[None], latent_grad[None], rope_grad[None], key_grad, value_grad)


def solution(mesh):
    return jax.shard_map(
        shards,
        mesh=mesh,
        in_specs=(
            P("dp", None, "sp"),
            P("dp", None, "sp"),
            P("dp", None, None),
            P("dp", None, None),
            P(),
            P("dp", "sp"),
            P("dp", "sp"),
        ),
        out_specs=(
            P("dp", None, "sp"),
            P("dp", None, None),
            P("dp", None, None),
            P("dp", "sp"),
            P("dp", "sp"),
        ),
        check_vma=False,
    )
```

time: 261 us -> 98.4 us (0.38)
  waiting for transfers between devices: 133 us -> 0 us
  Pallas kernels: 0 us -> 89.9 us
  blocking collectives: 60.2 us -> 0 us
  matrix products: 13.9 us -> 0 us
  between operations: 14.5 us -> 0.65 us
  other arithmetic: 13.3 us -> 0 us
  local copies, waits for them, and re-layouts: 19 us -> 7.59 us
  starting transfers between devices: 6.35 us -> 0 us
    psum x1 -> x0, waiting for transfers between devices: 133 us -> none  [in_one(): subtotal = lax.psum(flat, axis)]
    pallas_call x0 -> x1, Pallas kernels: none -> 89.9 us  [shards(): pl.pallas_call(kernel, out_shape=(jax.ShapeDtypeStruct((SEQ, 384), BF16),...]
    all_gather x1 -> x0, blocking collectives: 60.2 us -> none  [in_one_piece(): lax.all_gather(both, axis, axis=dim, tiled=True)]
    dot_general x15 -> x0, matrix products: 13.9 us -> none  [the longest x2 3.19 us: head_backward(): jnp.dot(head_grad, head_value.T, preferred_element_type=jnp.float32)]
    while x24 -> x0, local copies, waits for them, and re-layouts: 7.02 us -> none
    all_to_all x1 -> x0, starting transfers between devices: 6.32 us -> none  [sent_and_summed(): pieces = lax.all_to_all(cut_along(x, dim, peers), axis, 0, 0, tiled=True)]
    convert_element_type x8 -> x0, other arithmetic: 5.9 us -> none  [the longest x2 3.31 us: shards(): part.astype(jnp.float32)]
    unnamed x46 -> x12, local copies, waits for them, and re-layouts: 4.93 us -> 7.59 us
  transfers between devices with their start and end apart: 2 -> 0, of which waited for: 1 -> 0; matrix products, arithmetic and copies ran while one was open for 5% -> 0% of each run, Pallas kernels for 0% -> 0%
where the time goes in v1:
time: 98.4 us; the launch traced here: 98.1 us
  Pallas kernels  89.9 us (91%)
  local copies, waits for them, and re-layouts  7.59 us (8%)
    pallas_call x1, Pallas kernels, shards(): pl.pallas_call(kernel, out_shape=(jax.ShapeDtypeStruct((SEQ, 384), BF16),...  89.9 us
    unnamed x12, local copies, waits for them, and re-layouts  7.59 us

profile of v1, /device:TPU:6, one launch (start us, length us, event | category | flops | bytes accessed | tf_op | source)
XLA Modules:
  0.0 98.1 jit_solution(6100708568230064554)
XLA Ops:
  0.6 1.7 %copy.14 = bf16[1,768,64]{2,1,0:T(8,128)(2,1)} copy(bf16[1,768,64]{1,2,0:T(8,128)(2,1)} %param.12) | data formatting | bytes 196608 | tf_op args[3]
  2.3 89.9 %shard_map.128 = (bf16[768,384]{1,0:T(8,128)(2,1)}, bf16[768,512]{1,0:T(8,128)(2,1)}, bf16[768,64]{1,0:T(8,128)(2,1)}, f32[8,256]{1,0:T(8,128)}, f32[8,256]{1,0:T(8,128)}) custom-call(bf16[768,384]{1,0:T(8,128)(2,1)} %bitcast.12, bf16[768,256]{1,0:T(8,128)(2,1)} %bitcast.13, bf16[768,512]{1,0:T(8,128)(2,1)} %bitcast.10, bf16[768,64]{1,0:T(8,128)(2,1)} %bitcast.8, ...), custom_call_target="tpu_custom_call" | custom-call | tf_op jit(solution)/shard_map/pallas_call | solution.py:390
  92.2 0.0 copy-start
  92.2 1.8 %copy.15 = bf16[1,768,64]{1,2,0:T(8,128)(2,1)} copy(bf16[1,768,64]{2,1,0:T(8,128)(2,1)} %bitcast.14) | data formatting | bytes 196608
  94.0 1.9 %copy.20 = bf16[1,768,384]{2,1,0:T(8,128)(2,1)} copy(bf16[1,768,384]{2,1,0:T(8,128)(2,1)} %bitcast.11) | data formatting | bytes 1179648
  95.9 0.0 copy-done
  95.9 0.0 copy-start.2
  95.9 0.9 copy.21
  96.8 0.0 copy-done.2
  96.8 0.0 copy-start.1
  96.8 0.6 copy.22
  97.4 0.1 copy-done.1
  97.5 0.6 copy.23
Async XLA Ops:
  92.2 3.7 %copy-start = (bf16[768,512]{1,0:T(8,128)(2,1)S(1)}, bf16[768,512]{1,0:T(8,128)(2,1)}, u32[]{:S(2)}) copy-start(bf16[768,512]{1,0:T(8,128)(2,1)} %get-tuple-element.11) | copy-start | bytes 2359300
  95.9 0.9 copy-start.2
  96.8 0.7 copy-start.1
